TPU v7x, 32 devices: a whole 2x2x4 slice. The times are simulated.
32 devices in a mesh: sp: 8 (over z, y), tp: 4 (over x, core).
Axes of the slice: x: 2, y: 2, z: 4, core: 2. Of those that a mesh axis runs over, the one named last changes fastest.
Arguments:
- resid_stream: bfloat16 [3072, 2048], P('sp'), may hold values from -6 to 6
- q_latent: bfloat16 [3072, 512], P('sp'), may hold values from -6 to 6
- kv_latent: bfloat16 [3072, 256], P('sp'), may hold values from -6 to 6
- rope_key: bfloat16 [3072, 64], P('sp'), may hold values from -6 to 6
- doc_ids: int32 [3072], P('sp'), may hold values from 0 to 3, as said below
- q_gain: float32 [512], replicated, may hold values from 1.5 to 64
- kv_gain: float32 [256], replicated, may hold values from 0.1 to 1.9
- w_query: bfloat16 [512, 3072], P(None, 'tp'), may hold values from -0.25 to 0.25
- w_key: bfloat16 [256, 2048], P(None, 'tp'), may hold values from -0.375 to 0.375
- w_value: bfloat16 [256, 2048], P(None, 'tp'), may hold values from -0.375 to 0.375
- w_out: bfloat16 [2048, 2048], replicated, may hold values from -0.5 to 0.5
- mix_gain: float32 [2048], replicated, may hold values from 0.1 to 1.9
- w_gate: bfloat16 [2048, 5632], P('sp', 'tp'), may hold values from -0.125 to 0.125
- w_up: bfloat16 [2048, 5632], P('sp', 'tp'), may hold values from -0.125 to 0.125
- w_down: bfloat16 [5632, 2048], P('tp', 'sp'), may hold values from -0.3125 to 0.3125
- out_gain: float32 [2048], replicated, may hold values from 0.1 to 1.9
Outputs:
- layer_out: bfloat16 [3072, 2048], P(('sp', 'tp'))
Inputs may be any that keep to these rules, and one draw needn't show every extreme that they name: `doc_ids`: document numbers never fall along the sequence; every document has 1 to 2304 positions and one has exactly 2304.
All inputs are finite; a program needn't handle non-finite values.
Results may differ from a plain program's by a relative error of at most 0.02.
The roundings to bfloat16 on the way count: a program that leaves them out, or rounds other values in their place, can miss the bound.
Values may be sent and summed in bfloat16 or wider, within the bound.
A program may use at most 128 MiB of HBM per device.

v0:
```python
import jax
import jax.numpy as jnp
from jax import lax
from jax.sharding import PartitionSpec as P

NOPE = 128
RD = 64
VD = 128
eps_norm = 1e-05
rope_theta = 10000.0
resid_alpha = 8.0**0.25
key_span = 2048


def rope_angles(positions):
    frequency = rope_theta ** (-jnp.arange(0, RD, 2, dtype=jnp.float32) / RD)
    angles = positions.astype(jnp.float32)[:, None] * frequency[None, :]
    return (jnp.cos(angles), jnp.sin(angles))


def rotate(values, cos_table, sin_table):
    half_width = values.shape[-1] // 2
    first_half = values[..., :half_width]
    second_half = values[..., half_width:]
    return jnp.concatenate(
        [
            first_half * cos_table - second_half * sin_table,
            second_half * cos_table + first_half * sin_table,
        ],
        axis=-1,
    )


def rms_scaled(latent, scaling):
    widened = latent.astype(jnp.float32)
    inverse = lax.rsqrt(jnp.mean(widened * widened, axis=-1, keepdims=True) + eps_norm)
    return (widened * inverse * scaling).astype(jnp.bfloat16)


def layer_scaled(stream, scaling):
    centre = stream - jnp.mean(stream, axis=-1, keepdims=True)
    spread = jnp.mean(centre * centre, axis=-1, keepdims=True)
    return centre * lax.rsqrt(spread + eps_norm) * scaling


def fold_in_blocks(carried, piece_part, attend_fn):
    piece_rows = piece_part[0].shape[0]
    if piece_rows > key_span and piece_rows % key_span == 0:

        def one_block(inner, block_index):
            sliced = tuple(
                (
                    lax.dynamic_slice_in_dim(
                        member, (block_index * key_span).astype(jnp.int32), key_span, 0
                    )
                    for member in piece_part
                )
            )
            return (attend_fn(inner, sliced), None)

        outcome = lax.scan(one_block, carried, jnp.arange(piece_rows // key_span, dtype=jnp.int32))
        return outcome[0]
    return attend_fn(carried, piece_part)


def body(
    resid_stream,
    q_latent,
    kv_latent,
    rope_key,
    doc_ids,
    q_gain,
    kv_gain,
    w_query,
    w_key,
    w_value,
    w_out,
    mix_gain,
    w_gate,
    w_up,
    w_down,
    out_gain,
):
    tok_rows = q_latent.shape[0]
    head_count = w_key.shape[1] // NOPE
    tp_count = lax.axis_size("tp")
    part_rows = tok_rows // tp_count
    tp_index = lax.axis_index("tp")
    positions = lax.axis_index("sp") * tok_rows + jnp.arange(tok_rows, dtype=jnp.int32)
    cos_table, sin_table = rope_angles(positions)
    q_normed = rms_scaled(q_latent, q_gain)
    queries = jnp.dot(q_normed, w_query, preferred_element_type=jnp.float32).reshape(
        tok_rows, head_count, NOPE + RD
    )
    query_nope = queries[:, :, :NOPE].astype(jnp.bfloat16)
    query_rope = rotate(queries[:, :, NOPE:], cos_table[:, None, :], sin_table[:, None, :]).astype(
        jnp.bfloat16
    )
    kv_normed = rms_scaled(kv_latent, kv_gain)
    key_rot = rotate(rope_key.astype(jnp.float32), cos_table, sin_table).astype(jnp.bfloat16)
    score_scale = (NOPE + RD) ** (-0.5)

    def attend_rows(carried, piece_part):
        row_top, denom_sum, accum_out = carried
        key_piece, value_piece, rot_piece, doc_piece = piece_part
        piece_rows = key_piece.shape[0]
        keys_heads = key_piece.reshape(piece_rows, head_count, NOPE)
        values_heads = value_piece.reshape(piece_rows, head_count, VD)
        scores = jnp.einsum(
            "qhd,khd->hqk", query_nope, keys_heads, preferred_element_type=jnp.float32
        )
        scores = (
            scores
            + jnp.einsum("qhd,kd->hqk", query_rope, rot_piece, preferred_element_type=jnp.float32)
        ) * score_scale
        same_doc = (doc_ids[:, None] == doc_piece[None, :])[None]
        masked = jnp.where(same_doc, scores, -1e30)
        new_top = jnp.maximum(row_top, jnp.max(masked, axis=-1))
        weights = jnp.where(same_doc, jnp.exp(masked - new_top[:, :, None]), 0.0)
        factor = jnp.exp(row_top - new_top)
        denom_sum = denom_sum * factor + jnp.sum(weights, axis=-1)
        update = jnp.einsum(
            "hqk,khd->qhd",
            weights.astype(jnp.bfloat16),
            values_heads,
            preferred_element_type=jnp.float32,
        )
        accum_out = accum_out * jnp.transpose(factor)[:, :, None] + update
        return (new_top, denom_sum, accum_out)

    initial = (
        jnp.full((head_count, tok_rows), -1e30, jnp.float32),
        jnp.zeros((head_count, tok_rows), jnp.float32),
        jnp.zeros((tok_rows, head_count, VD), jnp.float32),
    )

    def project_rows(carried, piece_part):
        latent_piece, rot_piece, doc_piece = piece_part
        key_piece = jnp.dot(latent_piece, w_key, preferred_element_type=jnp.float32).astype(
            jnp.bfloat16
        )
        value_piece = jnp.dot(latent_piece, w_value, preferred_element_type=jnp.float32).astype(
            jnp.bfloat16
        )
        return attend_rows(carried, (key_piece, value_piece, rot_piece, doc_piece))

    carried_out = fold_in_blocks(
        initial,
        (
            lax.all_gather(kv_normed, "sp", axis=0, tiled=True),
            lax.all_gather(key_rot, "sp", axis=0, tiled=True),
            lax.all_gather(doc_ids, "sp", axis=0, tiled=True),
        ),
        project_rows,
    )
    denom_sum = carried_out[1]
    attended = (
        (carried_out[2] / jnp.transpose(denom_sum)[:, :, None])
        .astype(jnp.bfloat16)
        .reshape(tok_rows, head_count * VD)
    )
    heads_rows = lax.all_to_all(attended, "tp", split_axis=0, concat_axis=1, tiled=True)
    mixer_out = jnp.dot(heads_rows, w_out, preferred_element_type=jnp.float32)
    own_resid = lax.dynamic_slice_in_dim(resid_stream, tp_index * part_rows, part_rows, 0)
    own_normed = layer_scaled(
        resid_alpha * own_resid.astype(jnp.float32) + mixer_out, mix_gain
    ).astype(jnp.bfloat16)
    normed_rows = lax.all_gather(own_normed, "tp", axis=0, tiled=True)
    gate_part = jnp.dot(
        normed_rows,
        lax.all_gather(w_gate, "sp", axis=0, tiled=True),
        preferred_element_type=jnp.float32,
    )
    up_part = jnp.dot(
        normed_rows,
        lax.all_gather(w_up, "sp", axis=0, tiled=True),
        preferred_element_type=jnp.float32,
    )
    hidden = (jax.nn.silu(gate_part) * up_part).astype(jnp.bfloat16)
    down_term = jnp.dot(
        hidden, lax.all_gather(w_down, "sp", axis=1, tiled=True), preferred_element_type=jnp.float32
    )
    ffn_sum = lax.psum_scatter(
        down_term.astype(jnp.bfloat16), "tp", scatter_dimension=0, tiled=True
    ).astype(jnp.float32)
    layer_out = layer_scaled(
        resid_alpha * own_normed.astype(jnp.float32) + 0.5 * ffn_sum, out_gain
    ).astype(jnp.bfloat16)
    return layer_out


def solution(mesh):
    in_specs = (
        P("sp", None),
        P("sp", None),
        P("sp", None),
        P("sp", None),
        P("sp"),
        P(),
        P(),
        P(None, "tp"),
        P(None, "tp"),
        P(None, "tp"),
        P(),
        P(),
        P("sp", "tp"),
        P("sp", "tp"),
        P("tp", "sp"),
        P(),
    )
    out_specs = P(("sp", "tp"), None)
    return jax.shard_map(body, mesh=mesh, in_specs=in_specs, out_specs=out_specs, check_vma=False)
```

profile of v0, /device:TPU:0, one launch (start us, length us, event | category | flops | bytes accessed | tf_op | source)
XLA Modules:
  0.0 487.2 jit_solution(11520643036253584039)
XLA Ops:
  6.5 1.1 fusion.26
  7.7 1.7 fusion.28
  9.4 0.0 all-gather.7.cloned.1.call-update
  9.5 0.8 convert_element_type.64
  10.3 0.7 reshape.152
  11.0 27.9 %all-gather = s32[8,1,384]{2,1,0:T(1,128)S(1)} all-gather(s32[1,1,384]{2,1,0:T(1,128)S(1)} %reshape.152), channel_id=1, replica_groups=mesh['sp'=8,'tp'=4] {'sp'}, dimensions={0}, use_global_device_ids=true | all-gather | bytes 13824 | tf_op jit(solution)/shard_map/all_gather | solution.py:152
  38.9 0.3 multiply_cosine_fusion
  39.2 1.2 fusion.22
  40.3 32.1 %all_gather.23 = bf16[3072,64]{0,1:T(8,128)(2,1)S(1)} all-gather(bf16[384,64]{0,1:T(8,128)(2,1)S(1)} %pad_maximum_fusion), channel_id=1, replica_groups=mesh['sp'=8,'tp'=4] {'sp'}, dimensions={0}, use_global_device_ids=true | all-gather | bytes 442368 | tf_op jit(solution)/shard_map/all_gather | solution.py:151
  72.5 1.7 fusion.29
  74.2 0.1 subtract_convert_fusion
  74.2 0.7 broadcast_compare_fusion
  74.9 0.0 copy-start.3
  74.9 8.1 %fusion.31 = f32[3072,384,4]{0,1,2:T(8,128)} fusion(bf16[3072,64]{0,1:T(8,128)(2,1)S(1)} %all_gather.23, bf16[384,4,32]{0,2,1:T(8,128)(2,1)S(1)} %get-tuple-element.6, bf16[384,4,32]{0,2,1:T(8,128)(2,1)S(1)} %get-tuple-element.5), kind=kOutput, calls=%fused_computation.39 | convolution fusion | flops 604372992 | bytes 19464192 | tf_op jit(solution)/shard_map/qhd,kd->hqk/dot_general | solution.py:114
  83.0 2.4 convolution_convert_fusion.1
  85.5 12.7 %fusion.41 = (f32[4,384]{1,0:T(4,128)S(1)}, f32[4,384,3072]{2,1,0:T(8,128)}) fusion(f32[3072,384,4]{0,1,2:T(8,128)} %fusion.31, bf16[3072,4,128]{0,2,1:T(8,128)(2,1)S(1)} %bitcast.44, f32[384,4,192]{0,2,1:T(8,128)S(1)} %bitcast.47, pred[384,3072]{1,0:T(8,128)(4,1)S(1)} %broadcast_compare_fusion), kind=kOutput, calls=%fused_computation.67 | convolution fusion | flops 1226832384 | bytes 42473472 | tf_op jit(solution)/shard_map/qhd,khd->hqk/dot_general | solution.py:109
  98.2 0.0 copy-start.4
  98.2 9.0 %fusion.2 = f32[4,384]{1,0:T(4,128)S(1)} fusion(f32[4,384,3072]{2,1,0:T(8,128)} %get-tuple-element.16, f32[4,384]{1,0:T(4,128)S(1)} %get-tuple-element.10, pred[384,3072]{1,0:T(8,128)(4,1)S(1)} %broadcast_compare_fusion), kind=kLoop, calls=%fused_computation.4 | loop fusion | flops 14154240 | bytes 20066304 | tf_op jit(solution)/shard_map/reduce_sum | solution.py:121
  107.2 2.7 convolution_convert_fusion
  109.9 10.9 %fusion.19 = bf16[384,4,128]{0,2,1:T(8,128)(2,1)S(1)} fusion(bf16[3072,4,128]{0,2,1:T(8,128)(2,1)} %bitcast.45, f32[4,384,3072]{2,1,0:T(8,128)} %get-tuple-element.16, f32[4,384]{1,0:T(4,128)S(1)} %get-tuple-element.10, pred[384,3072]{1,0:T(8,128)(4,1)S(1)} %broadcast_compare_fusion, f32[384,4]{0,1:T(4,128)S(1)} %bitcast_add_fusion.1, ...), kind=kOutput, calls=%fused_computation.22 | convolution fusion | flops 1222705152 | bytes 23611392 | tf_op jit(solution)/shard_map/hqk,khd->qhd/dot_general | solution.py:122
  120.8 0.2 copy.38
  121.1 0.9 all_to_all.14
  122.0 3.5 all-to-all-start
  125.4 0.3 all-gather.9.cloned.1.call-start
  125.7 7.1 %all-to-all-done = bf16[4,96,512]{2,1,0:T(8,128)(2,1)S(1)} async-done(((bf16[4,96,512]{2,1,0:T(8,128)(2,1)}), bf16[4,96,512]{2,1,0:T(8,128)(2,1)S(1)}, u32[]{:S(2)}, u32[]{:S(2)}) %all-to-all-start) | async-done | bytes 393248 | tf_op jit(solution)/shard_map/all_to_all | solution.py:162
  132.8 0.0 copy-start.5
  132.9 5.0 %fusion.42 = (f32[96]{0:T(128)S(1)}, f32[96,2048]{1,0:T(8,128)S(1)}) fusion(bf16[96,2048]{1,0:T(8,128)(2,1)S(1)} %bitcast.48, bf16[2048,2048]{1,0:T(8,128)(2,1)} %param.26, bf16[384,2048]{1,0:T(8,128)(2,1)} %param.16, s32[]{:T(128)S(6)} %select_n.10), kind=kOutput, calls=%fused_computation.68 | convolution fusion | flops 806092672 | bytes 9961860 | tf_op jit(solution)/shard_map/dot_general | solution.py:163
  137.8 0.2 multiply_reduce_fusion.1
  138.1 0.9 multiply_convert_fusion.1
  139.0 0.0 all-gather.9.cloned.1.call-update
  139.1 0.0 all-gather.11.cloned.1.call-start
  139.1 0.7 all-gather.11.cloned.1.call-update
  139.8 0.0 all-gather.13.cloned.1.call-start
  139.8 0.5 all-gather.13.cloned.1.call-update
  140.4 0.0 all-gather.15.cloned.1.call-start
  140.4 0.5 all-gather.15.cloned.1.call-update
  141.0 0.0 reduce-scatter.2.cloned.1.call-start
  141.0 16.3 %all-gather.9.cloned.1.call-done = bf16[384,2048]{1,0:T(8,128)(2,1)} async-done(((bf16[96,2048]{1,0:T(8,128)(2,1)}), bf16[384,2048]{1,0:T(8,128)(2,1)}) %all-gather.9.cloned.1.call-update) | async-done | bytes 1572880 | tf_op jit(solution)/shard_map/all_gather | solution.py:168
  157.3 94.5 %all-gather.11.cloned.1.call-done = bf16[2048,1408]{1,0:T(8,128)(2,1)} async-done(((bf16[256,1408]{1,0:T(8,128)(2,1)}), bf16[2048,1408]{1,0:T(8,128)(2,1)}) %all-gather.11.cloned.1.call-update) | async-done | bytes 5767184 | tf_op jit(solution)/shard_map/all_gather | solution.py:171
  251.8 7.1 %fusion.43 = f32[384,1408]{1,0:T(8,128)} fusion(bf16[384,2048]{1,0:T(8,128)(2,1)} %all-gather.9.cloned.1.call-done, bf16[2048,1408]{1,0:T(8,128)(2,1)} %all-gather.11.cloned.1.call-done), kind=kOutput, calls=%fused_computation.69 | convolution fusion | flops 2214592512 | bytes 9502720 | tf_op jit(solution)/shard_map/dot_general | solution.py:169
  258.9 85.5 %all-gather.13.cloned.1.call-done = bf16[2048,1408]{1,0:T(8,128)(2,1)} async-done(((bf16[256,1408]{1,0:T(8,128)(2,1)}), bf16[2048,1408]{1,0:T(8,128)(2,1)}) %all-gather.13.cloned.1.call-update) | async-done | bytes 5767184 | tf_op jit(solution)/shard_map/all_gather | solution.py:176
  344.4 93.2 %all-gather.15.cloned.1.call-done = bf16[1408,2048]{1,0:T(8,128)(2,1)} async-done(((bf16[1408,256]{1,0:T(8,128)(2,1)}), bf16[1408,2048]{1,0:T(8,128)(2,1)}) %all-gather.15.cloned.1.call-update) | async-done | bytes 5767184 | tf_op jit(solution)/shard_map/all_gather | solution.py:181
  437.6 11.3 %convolution_convert_fusion.2 = bf16[384,2048]{1,0:T(8,128)(2,1)} fusion(bf16[1408,2048]{1,0:T(8,128)(2,1)} %all-gather.15.cloned.1.call-done, bf16[384,2048]{1,0:T(8,128)(2,1)S(1)} %copy-done.8, bf16[2048,1408]{1,0:T(8,128)(2,1)} %all-gather.13.cloned.1.call-done, f32[384,1408]{1,0:T(8,128)} %fusion.43), kind=kOutput, calls=%fused_computation.14 | convolution fusion | flops 4433215488 | bytes 16842752 | tf_op jit(solution)/shard_map/dot_general | solution.py:180
  448.9 0.0 reduce-scatter.2.cloned.1.call-update
  448.9 26.4 %reduce-scatter.2.cloned.1.call-done = bf16[96,2048]{1,0:T(8,128)(2,1)} async-done(((bf16[384,2048]{1,0:T(8,128)(2,1)}), bf16[96,2048]{1,0:T(8,128)(2,1)}) %reduce-scatter.2.cloned.1.call-update) | async-done | bytes 393232 | tf_op jit(solution)/shard_map/reduce_scatter | solution.py:183
  475.3 1.4 fusion.25
  476.7 1.4 multiply_reduce_fusion
  478.2 2.2 multiply_convert_fusion
  (29 shorter events, 0.1 us)
Async XLA Ops:
  6.5 65.9 %copy-start = (bf16[512,768]{1,0:T(8,128)(2,1)S(1)}, bf16[512,768]{1,0:T(8,128)(2,1)}, u32[]{:S(2)}) copy-start(bf16[512,768]{1,0:T(8,128)(2,1)} %param.23) | copy-start | bytes 2359300
  6.5 67.7 %copy-start.7 = (s32[384]{0:T(512)S(1)}, s32[384]{0:T(512)}, u32[]{:S(2)}) copy-start(s32[384]{0:T(512)} %param.20) | copy-start | bytes 4612
  6.5 76.5 %all-gather.7.cloned.1.call-start = ((), (), s32[]{:S(2)}) async-start(), calls=%async_computation.2 | async-start | bytes 1769472 | tf_op jit(solution)/shard_map/all_gather | solution.py:150
  74.9 8.1 %copy-start.3 = (bf16[256,512]{1,0:T(8,128)(2,1)S(1)}, bf16[256,512]{1,0:T(8,128)(2,1)}, u32[]{:S(2)}) copy-start(bf16[256,512]{1,0:T(8,128)(2,1)} %param.24) | copy-start | bytes 786436
  98.2 9.1 %copy-start.2 = (bf16[3072,256]{1,0:T(8,128)(2,1)S(1)}, bf16[3072,256]{1,0:T(8,128)(2,1)}, u32[]{:S(2)}) copy-start(bf16[3072,256]{1,0:T(8,128)(2,1)} %all-gather.7.cloned.1.call-done) | copy-start | bytes 4718596
  98.2 9.1 %copy-start.4 = (bf16[256,512]{1,0:T(8,128)(2,1)S(1)}, bf16[256,512]{1,0:T(8,128)(2,1)}, u32[]{:S(2)}) copy-start(bf16[256,512]{1,0:T(8,128)(2,1)} %param.25) | copy-start | bytes 786436
  122.0 10.8 %all-to-all-start = ((bf16[4,96,512]{2,1,0:T(8,128)(2,1)}), bf16[4,96,512]{2,1,0:T(8,128)(2,1)S(1)}, u32[]{:S(2)}, u32[]{:S(2)}) async-start(bf16[4,96,512]{2,1,0:T(8,128)(2,1)} %all_to_all.14), calls=%async_computation | async-start | bytes 786432 | tf_op jit(solution)/shard_map/all_to_all | solution.py:162
  125.4 31.8 %all-gather.9.cloned.1.call-start = ((), (), s32[]{:S(2)}) async-start(), calls=%async_computation.3 | async-start | bytes 1966080 | tf_op jit(solution)/shard_map/all_gather | solution.py:168
  132.8 5.3 %copy-start.5 = (f32[2048]{0:T(1024)S(1)}, f32[2048]{0:T(1024)}, u32[]{:S(2)}) copy-start(f32[2048]{0:T(1024)} %param.27) | copy-start | bytes 24580
  139.1 112.8 %all-gather.11.cloned.1.call-start = ((), (), s32[]{:S(2)}) async-start(), calls=%async_computation.4 | async-start | bytes 6488064 | tf_op jit(solution)/shard_map/all_gather | solution.py:171
  139.8 204.6 %all-gather.13.cloned.1.call-start = ((), (), s32[]{:S(2)}) async-start(), calls=%async_computation.5 | async-start | bytes 6488064 | tf_op jit(solution)/shard_map/all_gather | solution.py:176
  140.4 297.2 %all-gather.15.cloned.1.call-start = ((), (), s32[]{:S(2)}) async-start(), calls=%async_computation.6 | async-start | bytes 6488064 | tf_op jit(solution)/shard_map/all_gather | solution.py:181
  141.0 334.4 %reduce-scatter.2.cloned.1.call-start = ((), (), s32[]{:S(2)}) async-start(), calls=%async_computation.7 | async-start | bytes 1966080 | tf_op jit(solution)/shard_map/reduce_scatter | solution.py:183
  157.3 280.3 %copy-start.8 = (bf16[384,2048]{1,0:T(8,128)(2,1)S(1)}, bf16[384,2048]{1,0:T(8,128)(2,1)}, u32[]{:S(2)}) copy-start(bf16[384,2048]{1,0:T(8,128)(2,1)} %all-gather.9.cloned.1.call-done) | copy-start | bytes 4718596
  437.6 42.8 %copy-start.1 = (bf16[512,768]{1,0:T(8,128)(2,1)S(1)}, bf16[512,768]{1,0:T(8,128)(2,1)}, u32[]{:S(2)}) copy-start(bf16[512,768]{1,0:T(8,128)(2,1)} %param.23) | copy-start | bytes 2359300
  448.9 29.3 %copy-start.6 = (f32[2048]{0:T(1024)S(1)}, f32[2048]{0:T(1024)}, u32[]{:S(2)}) copy-start(f32[2048]{0:T(1024)} %param.31) | copy-start | bytes 24580
Sparse Core Ops, SparseCore 0:
  9.6 49.9 all-gather.6
  139.2 18.0 all-gather.8
  159.5 92.3 all-gather.10
  253.8 90.4 all-gather.12
  346.3 91.2 all-gather.14
  449.1 26.2 reduce-scatter.1
where the time goes:
time: 488 us; the launch traced here: 487 us
  waiting for transfers between devices  325 us (67%)
  matrix products  61.8 us (13%)
  blocking collectives  60 us (12%)
  other arithmetic  21.1 us (4%)
  between operations  13.7 us (3%)
    all_gather x1, waiting for transfers between devices, body(): lax.all_gather(w_gate, 'sp', axis=0, tiled=True)  94.5 us
    all_gather x1, waiting for transfers between devices, body(): lax.all_gather(w_down, 'sp', axis=1, tiled=True)  93.2 us
    all_gather x1, waiting for transfers between devices, body(): lax.all_gather(w_up, 'sp', axis=0, tiled=True)  85.5 us
    all_gather x1, blocking collectives, body(): lax.all_gather(key_rot, 'sp', axis=0, tiled=True)  32.1 us
    all_gather x1, blocking collectives, body(): lax.all_gather(doc_ids, 'sp', axis=0, tiled=True)  27.9 us
    reduce_scatter x1, waiting for transfers between devices, body(): lax.psum_scatter(down_term.astype(jnp.bfloat16), 'tp', scatter_dimension=...  26.4 us
    all_gather x1, waiting for transfers between devices, body(): normed_rows = lax.all_gather(own_normed, 'tp', axis=0, tiled=True)  16.3 us
    dot_general x1, matrix products, attend_rows(): jnp.einsum('qhd,khd->hqk', query_nope, keys_heads, preferred_element_type...  12.7 us
  transfers between devices with their start and end apart: 7, of which 6 were waited for; matrix products, arithmetic and copies ran while one was open for 4% of the time, Pallas kernels for 0%

commit v1 on v0

--- a/solution.py
+++ b/solution.py
@@ -10,6 +10,11 @@
 rope_theta = 10000.0
 resid_alpha = 8.0**0.25
 key_span = 2048
+
+
+def stack_and_merge(x, name, along):
+    tiles = lax.all_gather(x, name)
+    return jnp.concatenate(tiles, axis=along)
 
 
 def rope_angles(positions):
@@ -178,7 +183,7 @@
     )
     hidden = (jax.nn.silu(gate_part) * up_part).astype(jnp.bfloat16)
     down_term = jnp.dot(
-        hidden, lax.all_gather(w_down, "sp", axis=1, tiled=True), preferred_element_type=jnp.float32
+        hidden, stack_and_merge(w_down, "sp", 1), preferred_element_type=jnp.float32
     )
     ffn_sum = lax.psum_scatter(
         down_term.astype(jnp.bfloat16), "tp", scatter_dimension=0, tiled=True

time: 488 us -> 410 us (0.84)
  waiting for transfers between devices: 325 us -> 237 us
  local copies, waits for them, and re-layouts: 1.9 us -> 10.2 us
    all_gather x1, waiting for transfers between devices: 93.2 us -> 11.3 us  [stack_and_merge(): tiles = lax.all_gather(x, name)]
    reshape x0 -> x1, local copies, waits for them, and re-layouts: none -> 8.34 us  [stack_and_merge(): return jnp.concatenate(tiles, axis=along)]
    all_gather x1, waiting for transfers between devices: 16.3 us -> 11.1 us  [body(): normed_rows = lax.all_gather(own_normed, 'tp', axis=0, tiled=True)]
  transfers between devices with their start and end apart: 7 -> 7, of which waited for: 6 -> 6; matrix products, arithmetic and copies ran while one was open for 4% -> 18% of each run, Pallas kernels for 0% -> 0%
where the time goes in v1:
time: 410 us; the launch traced here: 409 us
  waiting for transfers between devices  237 us (58%)
  matrix products  61.9 us (15%)
  blocking collectives  60 us (15%)
  other arithmetic  21.8 us (5%)
  between operations  13.7 us (3%)
  local copies, waits for them, and re-layouts  10.2 us (2%)
    all_gather x1, waiting for transfers between devices, body(): lax.all_gather(w_gate, 'sp', axis=0, tiled=True)  94.4 us
    all_gather x1, waiting for transfers between devices, body(): lax.all_gather(w_up, 'sp', axis=0, tiled=True)  85.5 us
    all_gather x1, blocking collectives, body(): lax.all_gather(key_rot, 'sp', axis=0, tiled=True)  32.1 us
    all_gather x1, blocking collectives, body(): lax.all_gather(doc_ids, 'sp', axis=0, tiled=True)  27.9 us
    reduce_scatter x1, waiting for transfers between devices, body(): lax.psum_scatter(down_term.astype(jnp.bfloat16), 'tp', scatter_dimension=...  26.4 us
    dot_general x1, matrix products, attend_rows(): jnp.einsum('qhd,khd->hqk', query_nope, keys_heads, preferred_element_type...  12.6 us
    dot_general x1, matrix products, body(): jnp.dot(hidden, stack_and_merge(w_down, 'sp', 1), preferred_element_type=...  11.3 us
    all_gather x1, waiting for transfers between devices, stack_and_merge(): tiles = lax.all_gather(x, name)  11.3 us
  transfers between devices with their start and end apart: 7, of which 6 were waited for; matrix products, arithmetic and copies ran while one was open for 18% of the time, Pallas kernels for 0%

profile of v1, /device:TPU:0, one launch (start us, length us, event | category | flops | bytes accessed | tf_op | source)
XLA Modules:
  0.0 409.0 jit_solution(2798286982431660856)
XLA Ops:
  6.5 1.2 fusion.26
  7.7 1.7 fusion.28
  9.5 0.0 all-gather.8.cloned.1.call-update
  9.5 0.0 all-gather.16.cloned.1.call-start
  9.5 0.7 all-gather.16.cloned.1.call-update
  10.3 0.8 convert_element_type.64
  11.1 0.7 reshape.161
  11.7 27.9 %all-gather.1 = s32[8,1,384]{2,1,0:T(1,128)S(1)} all-gather(s32[1,1,384]{2,1,0:T(1,128)S(1)} %reshape.161), channel_id=1, replica_groups=mesh['sp'=8,'tp'=4] {'sp'}, dimensions={0}, use_global_device_ids=true | all-gather | bytes 13824 | tf_op jit(solution)/shard_map/all_gather | solution.py:157
  39.7 0.3 multiply_cosine_fusion
  40.0 1.2 fusion.22
  41.1 32.1 %all_gather.26 = bf16[3072,64]{0,1:T(8,128)(2,1)S(1)} all-gather(bf16[384,64]{0,1:T(8,128)(2,1)S(1)} %pad_maximum_fusion), channel_id=1, replica_groups=mesh['sp'=8,'tp'=4] {'sp'}, dimensions={0}, use_global_device_ids=true | all-gather | bytes 442368 | tf_op jit(solution)/shard_map/all_gather | solution.py:156
  73.2 1.4 fusion.29
  74.6 0.1 subtract_convert_fusion
  74.7 0.7 broadcast_compare_fusion
  75.4 8.2 %fusion.31 = f32[3072,384,4]{0,1,2:T(8,128)} fusion(bf16[3072,64]{0,1:T(8,128)(2,1)S(1)} %all_gather.26, bf16[384,4,32]{0,2,1:T(8,128)(2,1)S(1)} %get-tuple-element.6, bf16[384,4,32]{0,2,1:T(8,128)(2,1)S(1)} %get-tuple-element.5), kind=kOutput, calls=%fused_computation.39 | convolution fusion | flops 604372992 | bytes 19464192 | tf_op jit(solution)/shard_map/qhd,kd->hqk/dot_general | solution.py:119
  83.6 2.5 convolution_convert_fusion.1
  86.1 12.6 %fusion.41 = (f32[4,384]{1,0:T(4,128)S(1)}, f32[4,384,3072]{2,1,0:T(8,128)}) fusion(f32[3072,384,4]{0,1,2:T(8,128)} %fusion.31, bf16[3072,4,128]{0,2,1:T(8,128)(2,1)S(1)} %bitcast.48, f32[384,4,192]{0,2,1:T(8,128)S(1)} %bitcast.51, pred[384,3072]{1,0:T(8,128)(4,1)S(1)} %broadcast_compare_fusion), kind=kOutput, calls=%fused_computation.67 | convolution fusion | flops 1226832384 | bytes 42473472 | tf_op jit(solution)/shard_map/qhd,khd->hqk/dot_general | solution.py:114
  98.7 0.0 copy-start.5
  98.7 9.7 %fusion.2 = f32[4,384]{1,0:T(4,128)S(1)} fusion(f32[4,384,3072]{2,1,0:T(8,128)} %get-tuple-element.16, f32[4,384]{1,0:T(4,128)S(1)} %get-tuple-element.10, pred[384,3072]{1,0:T(8,128)(4,1)S(1)} %broadcast_compare_fusion), kind=kLoop, calls=%fused_computation.4 | loop fusion | flops 14154240 | bytes 20066304 | tf_op jit(solution)/shard_map/reduce_sum | solution.py:126
  108.4 2.8 convolution_convert_fusion
  111.2 10.9 %fusion.19 = bf16[384,4,128]{0,2,1:T(8,128)(2,1)S(1)} fusion(bf16[3072,4,128]{0,2,1:T(8,128)(2,1)} %bitcast.49, f32[4,384,3072]{2,1,0:T(8,128)} %get-tuple-element.16, f32[4,384]{1,0:T(4,128)S(1)} %get-tuple-element.10, pred[384,3072]{1,0:T(8,128)(4,1)S(1)} %broadcast_compare_fusion, f32[384,4]{0,1:T(4,128)S(1)} %bitcast_add_fusion.1, ...), kind=kOutput, calls=%fused_computation.22 | convolution fusion | flops 1222705152 | bytes 23611392 | tf_op jit(solution)/shard_map/hqk,khd->qhd/dot_general | solution.py:127
  122.1 0.2 copy.46
  122.4 0.9 all_to_all.14
  123.3 3.5 all-to-all-start
  126.7 0.3 all-gather.10.cloned.1.call-start
  127.0 7.1 %all-to-all-done = bf16[4,96,512]{2,1,0:T(8,128)(2,1)S(1)} async-done(((bf16[4,96,512]{2,1,0:T(8,128)(2,1)}), bf16[4,96,512]{2,1,0:T(8,128)(2,1)S(1)}, u32[]{:S(2)}, u32[]{:S(2)}) %all-to-all-start) | async-done | bytes 393248 | tf_op jit(solution)/shard_map/all_to_all | solution.py:167
  134.2 0.0 copy-start.6
  134.2 5.2 %fusion.42 = (f32[96]{0:T(128)S(1)}, f32[96,2048]{1,0:T(8,128)S(1)}) fusion(bf16[96,2048]{1,0:T(8,128)(2,1)S(1)} %bitcast.54, bf16[2048,2048]{1,0:T(8,128)(2,1)} %param.26, bf16[384,2048]{1,0:T(8,128)(2,1)} %param.16, s32[]{:T(128)S(6)} %select_n.10), kind=kOutput, calls=%fused_computation.68 | convolution fusion | flops 806092672 | bytes 9961860 | tf_op jit(solution)/shard_map/dot_general | solution.py:168
  139.4 0.2 multiply_reduce_fusion.1
  139.7 0.9 multiply_convert_fusion.1
  140.6 0.0 all-gather.10.cloned.1.call-update
  140.6 0.0 all-gather.12.cloned.1.call-start
  140.7 0.5 all-gather.12.cloned.1.call-update
  141.2 0.0 all-gather.14.cloned.1.call-start
  141.2 0.5 all-gather.14.cloned.1.call-update
  141.8 0.0 reduce-scatter.2.cloned.1.call-start
  141.8 11.3 %all-gather.16.cloned.1.call-done = bf16[11264,256]{1,0:T(8,128)(2,1)} async-done(((bf16[1408,256]{1,0:T(8,128)(2,1)}), bf16[11264,256]{1,0:T(8,128)(2,1)}) %all-gather.16.cloned.1.call-update) | async-done | bytes 5767184 | tf_op jit(solution)/shard_map/all_gather | solution.py:16
  153.1 8.3 %copy.48 = bf16[1408,8,256]{0,2,1:T(8,128)(2,1)} copy(bf16[1408,8,256]{2,0,1:T(8,128)(2,1)} %bitcast.52) | data formatting | bytes 11534336 | tf_op jit(solution)/shard_map/reshape | solution.py:17
  161.4 11.1 %all-gather.10.cloned.1.call-done = bf16[384,2048]{1,0:T(8,128)(2,1)} async-done(((bf16[96,2048]{1,0:T(8,128)(2,1)}), bf16[384,2048]{1,0:T(8,128)(2,1)}) %all-gather.10.cloned.1.call-update) | async-done | bytes 1572880 | tf_op jit(solution)/shard_map/all_gather | solution.py:173
  172.5 94.4 %all-gather.12.cloned.1.call-done = bf16[2048,1408]{1,0:T(8,128)(2,1)} async-done(((bf16[256,1408]{1,0:T(8,128)(2,1)}), bf16[2048,1408]{1,0:T(8,128)(2,1)}) %all-gather.12.cloned.1.call-update) | async-done | bytes 5767184 | tf_op jit(solution)/shard_map/all_gather | solution.py:176
  266.9 7.1 %fusion.43 = f32[384,1408]{1,0:T(8,128)} fusion(bf16[384,2048]{1,0:T(8,128)(2,1)} %all-gather.10.cloned.1.call-done, bf16[2048,1408]{1,0:T(8,128)(2,1)} %all-gather.12.cloned.1.call-done), kind=kOutput, calls=%fused_computation.69 | convolution fusion | flops 2214592512 | bytes 9502720 | tf_op jit(solution)/shard_map/dot_general | solution.py:174
  274.0 85.5 %all-gather.14.cloned.1.call-done = bf16[2048,1408]{1,0:T(8,128)(2,1)} async-done(((bf16[256,1408]{1,0:T(8,128)(2,1)}), bf16[2048,1408]{1,0:T(8,128)(2,1)}) %all-gather.14.cloned.1.call-update) | async-done | bytes 5767184 | tf_op jit(solution)/shard_map/all_gather | solution.py:181
  359.5 11.3 %convolution_convert_fusion.2 = bf16[384,2048]{1,0:T(8,128)(2,1)} fusion(bf16[1408,2048]{0,1:T(8,128)(2,1)} %bitcast.53, bf16[384,2048]{1,0:T(8,128)(2,1)S(1)} %copy-done.9, bf16[2048,1408]{1,0:T(8,128)(2,1)} %all-gather.14.cloned.1.call-done, f32[384,1408]{1,0:T(8,128)} %fusion.43), kind=kOutput, calls=%fused_computation.14 | convolution fusion | flops 4433215488 | bytes 16842752 | tf_op jit(solution)/shard_map/dot_general | solution.py:185
  370.7 0.0 reduce-scatter.2.cloned.1.call-update
  370.8 26.4 %reduce-scatter.2.cloned.1.call-done = bf16[96,2048]{1,0:T(8,128)(2,1)} async-done(((bf16[384,2048]{1,0:T(8,128)(2,1)}), bf16[96,2048]{1,0:T(8,128)(2,1)}) %reduce-scatter.2.cloned.1.call-update) | async-done | bytes 393232 | tf_op jit(solution)/shard_map/reduce_scatter | solution.py:188
  397.1 1.4 fusion.25
  398.5 1.4 multiply_reduce_fusion
  400.0 2.2 multiply_convert_fusion
  (32 shorter events, 0.2 us)
Async XLA Ops:
  6.5 66.7 %copy-start = (bf16[512,768]{1,0:T(8,128)(2,1)S(1)}, bf16[512,768]{1,0:T(8,128)(2,1)}, u32[]{:S(2)}) copy-start(bf16[512,768]{1,0:T(8,128)(2,1)} %param.23) | copy-start | bytes 2359300
  6.5 68.2 %copy-start.8 = (s32[384]{0:T(512)S(1)}, s32[384]{0:T(512)}, u32[]{:S(2)}) copy-start(s32[384]{0:T(512)} %param.20) | copy-start | bytes 4612
  6.5 66.7 %copy-start.3 = (bf16[384,512]{1,0:T(8,128)(2,1)S(1)}, bf16[384,512]{1,0:T(8,128)(2,1)}, u32[]{:S(2)}) copy-start(bf16[384,512]{1,0:T(8,128)(2,1)} %param.17) | copy-start | bytes 1179652
  6.5 77.1 %all-gather.8.cloned.1.call-start = ((), (), s32[]{:S(2)}) async-start(), calls=%async_computation.2 | async-start | bytes 1769472 | tf_op jit(solution)/shard_map/all_gather | solution.py:155
  9.5 143.6 %all-gather.16.cloned.1.call-start = ((), (), s32[]{:S(2)}) async-start(), calls=%async_computation.7 | async-start | bytes 6488064 | tf_op jit(solution)/shard_map/all_gather | solution.py:16
  75.4 8.2 %copy-start.4 = (bf16[256,512]{1,0:T(8,128)(2,1)S(1)}, bf16[256,512]{1,0:T(8,128)(2,1)}, u32[]{:S(2)}) copy-start(bf16[256,512]{1,0:T(8,128)(2,1)} %param.24) | copy-start | bytes 786436
  98.7 9.7 %copy-start.2 = (bf16[3072,256]{1,0:T(8,128)(2,1)S(1)}, bf16[3072,256]{1,0:T(8,128)(2,1)}, u32[]{:S(2)}) copy-start(bf16[3072,256]{1,0:T(8,128)(2,1)} %all-gather.8.cloned.1.call-done) | copy-start | bytes 4718596
  98.7 9.7 %copy-start.5 = (bf16[256,512]{1,0:T(8,128)(2,1)S(1)}, bf16[256,512]{1,0:T(8,128)(2,1)}, u32[]{:S(2)}) copy-start(bf16[256,512]{1,0:T(8,128)(2,1)} %param.25) | copy-start | bytes 786436
  123.3 10.8 %all-to-all-start = ((bf16[4,96,512]{2,1,0:T(8,128)(2,1)}), bf16[4,96,512]{2,1,0:T(8,128)(2,1)S(1)}, u32[]{:S(2)}, u32[]{:S(2)}) async-start(bf16[4,96,512]{2,1,0:T(8,128)(2,1)} %all_to_all.14), calls=%async_computation | async-start | bytes 786432 | tf_op jit(solution)/shard_map/all_to_all | solution.py:167
  126.7 45.8 %all-gather.10.cloned.1.call-start = ((), (), s32[]{:S(2)}) async-start(), calls=%async_computation.3 | async-start | bytes 1966080 | tf_op jit(solution)/shard_map/all_gather | solution.py:173
  134.2 5.5 %copy-start.6 = (f32[2048]{0:T(1024)S(1)}, f32[2048]{0:T(1024)}, u32[]{:S(2)}) copy-start(f32[2048]{0:T(1024)} %param.27) | copy-start | bytes 24580
  140.6 126.3 %all-gather.12.cloned.1.call-start = ((), (), s32[]{:S(2)}) async-start(), calls=%async_computation.4 | async-start | bytes 6488064 | tf_op jit(solution)/shard_map/all_gather | solution.py:176
  141.2 218.3 %all-gather.14.cloned.1.call-start = ((), (), s32[]{:S(2)}) async-start(), calls=%async_computation.5 | async-start | bytes 6488064 | tf_op jit(solution)/shard_map/all_gather | solution.py:181
  141.8 255.3 %reduce-scatter.2.cloned.1.call-start = ((), (), s32[]{:S(2)}) async-start(), calls=%async_computation.6 | async-start | bytes 1966080 | tf_op jit(solution)/shard_map/reduce_scatter | solution.py:188
  172.5 186.9 %copy-start.9 = (bf16[384,2048]{1,0:T(8,128)(2,1)S(1)}, bf16[384,2048]{1,0:T(8,128)(2,1)}, u32[]{:S(2)}) copy-start(bf16[384,2048]{1,0:T(8,128)(2,1)} %all-gather.10.cloned.1.call-done) | copy-start | bytes 4718596
  359.5 42.7 %copy-start.1 = (bf16[512,768]{1,0:T(8,128)(2,1)S(1)}, bf16[512,768]{1,0:T(8,128)(2,1)}, u32[]{:S(2)}) copy-start(bf16[512,768]{1,0:T(8,128)(2,1)} %param.23) | copy-start | bytes 2359300
  370.7 29.2 %copy-start.7 = (f32[2048]{0:T(1024)S(1)}, f32[2048]{0:T(1024)}, u32[]{:S(2)}) copy-start(f32[2048]{0:T(1024)} %param.31) | copy-start | bytes 24580
Sparse Core Ops, SparseCore 0:
  9.6 49.6 all-gather.7
  61.5 91.5 all-gather.15
  154.7 17.7 all-gather.9
  174.5 92.3 all-gather.11
  268.9 90.4 all-gather.13
  370.9 26.1 reduce-scatter.1
